TPU v7x, 32 devices: a whole 2x2x4 slice. The times are simulated.
32 devices in a mesh: ep: 8 (over z, core), tp: 4 (over y, x).
Axes of the slice: x: 2, y: 2, z: 4, core: 2. Of those that a mesh axis runs over, the one named last changes fastest.
Arguments:
- queries: bfloat16 [2048, 4096], P('ep', 'tp'), may hold values from -6 to 6
- keys: bfloat16 [2048, 1024], P('ep', 'tp'), may hold values from -6 to 6
- values: bfloat16 [2048, 1024], P('ep', 'tp'), may hold values from -6 to 6
- query_gain: float32 [64], replicated, may hold values from 1 to 11
- key_gain: float32 [64], replicated, may hold values from 1 to 11
- moe_rows: bfloat16 [2048, 4096], P('ep', 'tp'), may hold values from -14 to 14
- route_ids: int32 [2048, 2], P('ep'), may hold values from 0 to 7, all different within a row; in each aligned block of 256 rows (0 to 255, 256 to 511, ...) at most 96 rows name the same one
- group_weight: float32 [2048], P('ep'), may hold values from 0.2 to 1
- expert_weight: float32 [2048, 2], P('ep'), may hold values from 0.05 to 1
- expert_gate: bfloat16 [8, 4096, 2048], P('ep', None, 'tp'), may hold values from -0.09375 to 0.09375
- expert_up: bfloat16 [8, 4096, 2048], P('ep', None, 'tp'), may hold values from -0.09375 to 0.09375
- expert_down: bfloat16 [8, 2048, 4096], P('ep', None, 'tp'), may hold values from -0.125 to 0.125
Outputs:
- attended: bfloat16 [2048, 4096], P('ep', 'tp')
- moe_out: bfloat16 [2048, 4096], P('ep', 'tp')
Inputs may be any that keep to these rules, and one draw needn't show every extreme that they name: `route_ids`: each row names 2 different experts. Among the rows of one device no expert is named by more than 96 rows, and in every draw some expert is named by exactly 96 of them.
All inputs are finite; a program needn't handle non-finite values.
Results may differ from a plain program's by a relative error of at most 0.0055.
The roundings to bfloat16 on the way count: a program that leaves them out, or rounds other values in their place, can miss the bound.
Values may be sent and summed in bfloat16 or wider, within the bound.
A program may use at most 128 MiB of HBM per device.

v0:
```python
import jax
import jax.numpy as jnp
from jax import lax
from jax.sharding import PartitionSpec as P

D = 4096
HEAD_DIM = 64
GRID_W = 64
TOPK = 2


def rotary_tables(position):
    pair_count = HEAD_DIM // 4
    grid_pos = jnp.stack([position // GRID_W, position % GRID_W], axis=-1).astype(jnp.float32)
    frequency = 10000.0 ** (-jnp.arange(pair_count, dtype=jnp.float32) / pair_count)
    angles = grid_pos[:, :, None] * frequency
    return (jnp.cos(angles), jnp.sin(angles))


def normed_rotated(rows_in, gain, cosine, sine_of):
    row_count, head_count = (rows_in.shape[0], rows_in.shape[1])
    pair_count = HEAD_DIM // 4
    scaled = rows_in * lax.rsqrt(jnp.mean(rows_in * rows_in, axis=-1, keepdims=True) + 1e-06) * gain
    parted = scaled.reshape(row_count, head_count, 2, 2, pair_count)
    first_half, second = (parted[:, :, :, 0, :], parted[:, :, :, 1, :])
    cos_b, sin_b = (cosine[:, None], sine_of[:, None])
    turned = jnp.stack(
        [first_half * cos_b - second * sin_b, second * cos_b + first_half * sin_b], axis=3
    )
    return turned.reshape(row_count, head_count, HEAD_DIM).astype(jnp.bfloat16)


def attend_block(carried, portion, query_rot, kv_width):
    running_max, denominator, summed = carried
    key_count = portion.shape[0]
    head_count = kv_width // HEAD_DIM
    keys_part = portion[:, :kv_width].reshape(key_count, head_count, HEAD_DIM)
    values_part = portion[:, kv_width:].reshape(key_count, head_count, HEAD_DIM)
    scores = jnp.einsum(
        "tkgd,skd->kgts", query_rot, keys_part, preferred_element_type=jnp.float32
    ) * HEAD_DIM ** (-0.5)
    new_max = jnp.max(scores, axis=-1)
    factor = jnp.exp(running_max - new_max)
    weights = jnp.exp(scores - new_max[..., None])
    denominator = denominator * factor + jnp.sum(weights, axis=-1)
    summed = summed * factor[..., None] + jnp.einsum(
        "kgts,skd->kgtd",
        weights.astype(jnp.bfloat16),
        values_part,
        preferred_element_type=jnp.float32,
    )
    return (new_max, denominator, summed)


def on_device(
    queries,
    keys,
    values,
    query_gain,
    key_gain,
    moe_rows,
    route_ids,
    group_weight,
    expert_weight,
    expert_gate,
    expert_up,
    expert_down,
):
    tok_rows = queries.shape[0]
    q_heads = queries.shape[1] // HEAD_DIM
    k_heads = keys.shape[1] // HEAD_DIM
    group_size = q_heads // k_heads
    position = lax.axis_index("ep") * tok_rows + jnp.arange(tok_rows, dtype=jnp.int32)
    cosine, sine_of = rotary_tables(position)
    query_rot = normed_rotated(
        queries.astype(jnp.float32).reshape(tok_rows, q_heads, HEAD_DIM),
        query_gain,
        cosine,
        sine_of,
    )
    query_rot = query_rot.reshape(tok_rows, k_heads, group_size, HEAD_DIM)
    key_rot = normed_rotated(
        keys.astype(jnp.float32).reshape(tok_rows, k_heads, HEAD_DIM), key_gain, cosine, sine_of
    )
    kv_width = k_heads * HEAD_DIM
    joined = jnp.concatenate([key_rot.reshape(tok_rows, kv_width), values], axis=1)
    initial = (
        jnp.full((k_heads, group_size, tok_rows), -jnp.inf, jnp.float32),
        jnp.zeros((k_heads, group_size, tok_rows), jnp.float32),
        jnp.zeros((k_heads, group_size, tok_rows, HEAD_DIM), jnp.float32),
    )
    final_max, denominator, summed = attend_block(
        initial, lax.all_gather(joined, "ep", axis=0, tiled=True), query_rot, kv_width
    )
    attended = (
        (summed / denominator[..., None])
        .transpose(2, 0, 1, 3)
        .reshape(tok_rows, q_heads * HEAD_DIM)
        .astype(jnp.bfloat16)
    )
    moe_tokens = moe_rows.shape[0]
    local_experts = expert_gate.shape[0]
    expert_count = local_experts * lax.axis_size("ep")
    capacity = 3 * moe_tokens * TOPK // (2 * expert_count)
    picks = moe_tokens * TOPK
    route_list = route_ids.reshape(picks)
    one_hot = (route_list[:, None] == jnp.arange(expert_count, dtype=jnp.int32)[None, :]).astype(
        jnp.int32
    )
    rank_of = jnp.sum((jnp.cumsum(one_hot, axis=0) - one_hot) * one_hot, axis=1)
    slot_of = route_list * capacity + rank_of
    owner_of = (
        jnp.full((expert_count * capacity,), moe_tokens, jnp.int32)
        .at[slot_of]
        .set(jnp.arange(picks, dtype=jnp.int32) // TOPK)
    )
    padded = jnp.concatenate([moe_rows, jnp.zeros((1, moe_rows.shape[1]), moe_rows.dtype)], axis=0)
    arrived = lax.all_to_all(
        padded[owner_of].reshape(expert_count, capacity, moe_rows.shape[1]),
        "ep",
        split_axis=0,
        concat_axis=1,
        tiled=True,
    )
    portion = lax.all_gather(arrived, "tp", axis=2, tiled=True)
    widened = portion.astype(jnp.float32)
    gate_act = jnp.einsum("erd,edf->erf", portion, expert_gate, preferred_element_type=jnp.float32)
    up_act = jnp.einsum("erd,edf->erf", portion, expert_up, preferred_element_type=jnp.float32)
    square_sum = jnp.sum(widened * widened, axis=2)
    inv_rms = lax.rsqrt(square_sum / D + 1e-06)[..., None]
    hidden = (jax.nn.silu(gate_act * inv_rms) * (up_act * inv_rms)).astype(jnp.bfloat16)
    out_cols = expert_down.shape[2]
    expert_result = jnp.einsum(
        "erf,efd->erd",
        lax.all_gather(hidden, "tp", axis=2, tiled=True),
        expert_down,
        preferred_element_type=jnp.float32,
    ).astype(jnp.bfloat16)
    returned = lax.all_to_all(expert_result, "ep", split_axis=1, concat_axis=0, tiled=True)
    flat_back = returned.reshape(expert_count * capacity, out_cols)
    picked = flat_back[slot_of].reshape(moe_tokens, TOPK, out_cols).astype(jnp.float32)
    mixing = group_weight[:, None] * expert_weight / jnp.sum(expert_weight, axis=1, keepdims=True)
    moe_out = jnp.sum(mixing[:, :, None] * picked, axis=1).astype(jnp.bfloat16)
    return (attended, moe_out)


def solution(mesh):
    placed = (
        P("ep", "tp"),
        P("ep", "tp"),
        P("ep", "tp"),
        P(),
        P(),
        P("ep", "tp"),
        P("ep", None),
        P("ep"),
        P("ep", None),
        P("ep", None, "tp"),
        P("ep", None, "tp"),
        P("ep", None, "tp"),
    )
    return jax.shard_map(
        on_device,
        mesh=mesh,
        in_specs=placed,
        out_specs=(P("ep", "tp"), P("ep", "tp")),
        check_vma=False,
    )
```

profile of v0, /device:TPU:0, one launch (start us, length us, event | category | flops | bytes accessed | tf_op | source)
XLA Modules:
  0.0 295.3 jit_solution(2823822702659321500)
XLA Ops:
  7.2 0.7 broadcast_multiply_fusion
  7.9 0.8 copy.47
  9.3 1.1 reduce-window.6
  10.8 2.4 scatter_custom_fusion
  13.3 1.1 concatenate.11
  14.4 2.8 gather_fusion
  17.2 44.2 %all_to_all.21 = bf16[8,96,1024]{2,1,0:T(8,128)(2,1)} all-to-all(bf16[8,96,1024]{2,1,0:T(8,128)(2,1)S(1)} %bitcast.104), channel_id=1, replica_groups=mesh['ep'=8,'tp'=4] {'ep'}, dimensions={0} | all-to-all | bytes 3145728 | tf_op jit(solution)/shard_map/all_to_all | solution.py:118
  62.3 0.7 pad_maximum_fusion.1
  63.1 0.5 all-gather.9.cloned.1.call-start
  63.6 67.0 %all-gather.7.cloned.1.call-done = bf16[1,768,4096]{2,1,0:T(8,128)(2,1)} async-done(((bf16[1,768,1024]{2,1,0:T(8,128)(2,1)}), bf16[1,768,4096]{2,1,0:T(8,128)(2,1)}) %all-gather.7.cloned.1.call-update) | async-done | bytes 6291472 | tf_op jit(solution)/shard_map/all_gather | solution.py:125
  130.6 4.2 %multiply_reduce_fusion = f32[768]{0:T(1024)S(1)} fusion(bf16[1,768,4096]{2,1,0:T(8,128)(2,1)} %all-gather.7.cloned.1.call-done), kind=kLoop, calls=%fused_computation.9 | loop fusion | flops 9436416 | bytes 6294528 | tf_op jit(solution)/shard_map/reduce_sum | solution.py:129
  135.2 5.5 %fusion.5 = f32[768,512]{1,0:T(8,128)S(1)} fusion(bf16[1,768,4096]{2,1,0:T(8,128)(2,1)S(1)} %copy-done, bf16[1,4096,512]{2,1,0:T(8,128)(2,1)} %param.22), kind=kOutput, calls=%fused_computation.10 | convolution fusion | flops 3221225472 | bytes 12058624 | tf_op jit(solution)/shard_map/erd,edf->erf/dot_general | solution.py:128
  140.8 4.6 %multiply_convert_fusion = bf16[768,512]{1,0:T(8,128)(2,1)} fusion(f32[768,512]{1,0:T(8,128)S(1)} %fusion.5, bf16[1,4096,512]{2,1,0:T(8,128)(2,1)S(1)} %copy-done.9, bf16[1,768,4096]{2,1,0:T(8,128)(2,1)S(1)} %copy-done, f32[768]{0:T(1024)S(1)} %add_rsqrt_fusion.1), kind=kOutput, calls=%fused_computation.21 | convolution fusion | flops 3224371200 | bytes 12848128 | tf_op jit(solution)/shard_map/erd,edf->erf/dot_general | solution.py:127
  146.5 16.9 %all-gather.5.cloned.1.call-done = bf16[2048,512]{0,1:T(8,128)(2,1)} async-done(((bf16[256,512]{0,1:T(8,128)(2,1)}), bf16[2048,512]{0,1:T(8,128)(2,1)}) %all-gather.5.cloned.1.call-update) | async-done | bytes 2097168 | tf_op jit(solution)/shard_map/all_gather | solution.py:93
  163.4 2.7 fusion.44
  166.1 13.9 %bitcast_reduce_fusion = (f32[4,4,256]{2,1,0:T(4,128)S(1)}, f32[4,2048,256,4]{2,1,3,0:T(8,128)}) fusion(bf16[2048,4,64,1]{0,2,3,1:T(8,128)(2,1)S(1)} %bitcast.107, bf16[256,4,4,64]{0,3,2,1:T(8,128)(2,1)S(1)} %bitcast.108), kind=kOutput, calls=%fused_computation.4 | convolution fusion | flops 1090514944 | bytes 35143680 | tf_op jit(solution)/shard_map/tkgd,skd->kgts/dot_general | solution.py:39
  180.1 27.9 %all-gather.9.cloned.1.call-done = bf16[768,2048]{1,0:T(8,128)(2,1)} async-done(((bf16[768,512]{1,0:T(8,128)(2,1)}), bf16[768,2048]{1,0:T(8,128)(2,1)}) %all-gather.9.cloned.1.call-update) | async-done | bytes 3145744 | tf_op jit(solution)/shard_map/all_gather | solution.py:135
  208.0 6.6 %fusion.16 = bf16[1,768,1024]{2,1,0:T(8,128)(2,1)S(1)} fusion(bf16[768,2048]{1,0:T(8,128)(2,1)} %all-gather.9.cloned.1.call-done, bf16[1,2048,1024]{2,1,0:T(8,128)(2,1)} %param.23), kind=kOutput, calls=%fused_computation.22 | convolution fusion | flops 3222011904 | bytes 8912896 | tf_op jit(solution)/shard_map/erf,efd->erd/dot_general | solution.py:133
  214.5 2.4 copy.58
  217.0 0.5 broadcast.321
  217.5 11.2 %reduce.3 = bf16[768,1024]{1,0:T(8,128)(2,1)} reduce(bf16[768,1,1024]{2,1,0:T(2,128)(2,1)S(1)} %bitcast.101, bf16[]{:T(256)} %broadcast.321), dimensions={1}, to_apply=%bitcast.99.reduce_sub_computation | reduce | bytes 3145730
  228.7 4.1 %reshape.311 = bf16[8,2,49152]{2,1,0:T(2,128)(2,1)} reshape(bf16[768,1024]{1,0:T(8,128)(2,1)} %reduce.3) | data formatting | bytes 3145728
  232.8 4.6 %all-to-all-start.1 = ((bf16[8,2,49152]{2,1,0:T(2,128)(2,1)}), bf16[8,2,49152]{2,1,0:T(2,128)(2,1)S(1)}, u32[]{:S(2)}, u32[]{:S(2)}) async-start(bf16[8,2,49152]{2,1,0:T(2,128)(2,1)} %reshape.311), calls=%async_computation.1 | async-start | bytes 3145728 | tf_op jit(solution)/shard_map/all_to_all | solution.py:139
  237.4 13.6 %fusion.1 = f32[4,4,256]{2,1,0:T(4,128)S(1)} fusion(f32[4,2048,256,4]{2,1,3,0:T(8,128)} %get-tuple-element.19, f32[4,4,256]{2,1,0:T(4,128)S(1)} %get-tuple-element.18), kind=kLoop, calls=%fused_computation.6 | loop fusion | flops 25161728 | bytes 33587200 | tf_op jit(solution)/shard_map/reduce_sum | solution.py:45
  251.1 13.6 %fusion.32 = bf16[256,4,4,64]{0,3,2,1:T(8,128)(2,1)S(1)} fusion(bf16[2048,4,64,1]{0,2,3,1:T(8,128)(2,1)S(1)} %bitcast.106, f32[4,2048,256,4]{2,1,3,0:T(8,128)} %get-tuple-element.19, f32[4,4,256]{2,1,0:T(4,128)S(1)} %get-tuple-element.18, f32[256,4,4]{0,2,1:T(4,128)S(1)} %bitcast_add_fusion, f32[256,4,4]{0,2,1:T(4,128)S(1)} %multiply_bitcast_fusion), kind=kOutput, calls=%fused_computation.26 | convolution fusion | flops 1099694080 | bytes 35176448 | tf_op jit(solution)/shard_map/kgts,skd->kgtd/dot_general | solution.py:46
  264.7 1.0 copy.50
  265.7 9.5 %all-to-all-done.1 = bf16[8,2,49152]{2,1,0:T(2,128)(2,1)S(1)} async-done(((bf16[8,2,49152]{2,1,0:T(2,128)(2,1)}), bf16[8,2,49152]{2,1,0:T(2,128)(2,1)S(1)}, u32[]{:S(2)}, u32[]{:S(2)}) %all-to-all-start.1) | async-done | bytes 1572896 | tf_op jit(solution)/shard_map/all_to_all | solution.py:139
  275.2 3.9 %reshape.312 = bf16[768,1,1024]{2,1,0:T(2,128)(2,1)} reshape(bf16[8,2,49152]{2,1,0:T(2,128)(2,1)S(1)} %all-to-all-done.1) | data formatting | bytes 3145728
  279.1 2.5 copy.57
  281.6 2.1 gather_fusion.1
  283.7 1.3 reshape.278
  285.0 3.5 %multiply_reduce_fusion.1 = bf16[256,1024]{1,0:T(8,128)(2,1)} fusion(f32[256,2,1024]{2,1,0:T(2,128)S(1)} %reshape.278, f32[256,2]{1,0:T(8,128)S(1)} %copy.45), kind=kLoop, calls=%fused_computation.18 | loop fusion | flops 786432 | bytes 2623488 | tf_op jit(solution)/shard_map/reduce_sum | solution.py:143
  (64 shorter events, 3.2 us)
Async XLA Ops:
  7.2 123.4 %all-gather.7.cloned.1.call-start = ((), (), s32[]{:S(2)}) async-start(), calls=%async_computation.3 | async-start | bytes 7864320 | tf_op jit(solution)/shard_map/all_gather | solution.py:125
  17.2 44.3 %copy-start.3 = (bf16[256,256]{1,0:T(8,128)(2,1)S(1)}, bf16[256,256]{1,0:T(8,128)(2,1)}, u32[]{:S(2)}) copy-start(bf16[256,256]{1,0:T(8,128)(2,1)} %param.14) | copy-start | bytes 393220
  17.2 44.4 %copy-start.7 = (f32[64]{0:T(128)S(1)}, f32[64]{0:T(128)}, u32[]{:S(2)}) copy-start(f32[64]{0:T(128)} %param.16) | copy-start | bytes 772
  17.2 44.5 %copy-start.4 = (bf16[256,256]{1,0:T(8,128)(2,1)S(1)}, bf16[256,256]{1,0:T(8,128)(2,1)}, u32[]{:S(2)}) copy-start(bf16[256,256]{1,0:T(8,128)(2,1)} %param.13) | copy-start | bytes 393220
  61.5 101.9 %all-gather.5.cloned.1.call-start = ((), (), s32[]{:S(2)}) async-start(), calls=%async_computation.2 | async-start | bytes 2359296 | tf_op jit(solution)/shard_map/all_gather | solution.py:93
  63.1 144.9 %all-gather.9.cloned.1.call-start = ((), (), s32[]{:S(2)}) async-start(), calls=%async_computation.4 | async-start | bytes 3932160 | tf_op jit(solution)/shard_map/all_gather | solution.py:135
  130.6 4.6 %copy-start = (bf16[1,768,4096]{2,1,0:T(8,128)(2,1)S(1)}, bf16[1,768,4096]{2,1,0:T(8,128)(2,1)}, u32[]{:S(2)}) copy-start(bf16[1,768,4096]{2,1,0:T(8,128)(2,1)} %all-gather.7.cloned.1.call-done) | copy-start | bytes 18874372
  135.2 5.5 %copy-start.9 = (bf16[1,4096,512]{2,1,0:T(8,128)(2,1)S(1)}, bf16[1,4096,512]{2,1,0:T(8,128)(2,1)}, u32[]{:S(2)}) copy-start(bf16[1,4096,512]{2,1,0:T(8,128)(2,1)} %param.21) | copy-start | bytes 12582916
  140.7 4.7 %copy-start.8 = (f32[64]{0:T(128)S(1)}, f32[64]{0:T(128)}, u32[]{:S(2)}) copy-start(f32[64]{0:T(128)} %param.15) | copy-start | bytes 772
  140.7 4.8 %copy-start.2 = (bf16[256,1024]{1,0:T(8,128)(2,1)S(1)}, bf16[256,1024]{1,0:T(8,128)(2,1)}, u32[]{:S(2)}) copy-start(bf16[256,1024]{1,0:T(8,128)(2,1)} %param.12) | copy-start | bytes 1572868
  140.8 5.0 %copy-start.5 = (f32[256,2]{0,1:T(2,128)S(1)}, f32[256,2]{0,1:T(2,128)}, u32[]{:S(2)}) copy-start(f32[256,2]{0,1:T(2,128)} %param.20) | copy-start | bytes 6148
  140.8 5.0 %copy-start.6 = (f32[256]{0:T(256)S(1)}, f32[256]{0:T(256)}, u32[]{:S(2)}) copy-start(f32[256]{0:T(256)} %param.19) | copy-start | bytes 3076
  232.8 42.4 %all-to-all-start.1 = ((bf16[8,2,49152]{2,1,0:T(2,128)(2,1)}), bf16[8,2,49152]{2,1,0:T(2,128)(2,1)S(1)}, u32[]{:S(2)}, u32[]{:S(2)}) async-start(bf16[8,2,49152]{2,1,0:T(2,128)(2,1)} %reshape.311), calls=%async_computation.1 | async-start | bytes 3145728 | tf_op jit(solution)/shard_map/all_to_all | solution.py:139
  237.4 13.7 %copy-start.1 = (bf16[2048,256]{0,1:T(8,128)(2,1)S(1)}, bf16[2048,256]{0,1:T(8,128)(2,1)}, u32[]{:S(2)}) copy-start(bf16[2048,256]{0,1:T(8,128)(2,1)} %get-tuple-element.11) | copy-start | bytes 3145732
Sparse Core Ops, SparseCore 0:
  61.6 68.9 all-gather.6
  132.7 30.5 all-gather.4
  165.2 42.7 all-gather.8
where the time goes:
time: 299 us; the launch traced here: 295 us
  waiting for transfers between devices  121 us (40%)
  blocking collectives  44.2 us (15%)
  matrix products  44.2 us (15%)
  other arithmetic  36.3 us (12%)
  local copies, waits for them, and re-layouts  29.7 us (10%)
  between operations  14.4 us (5%)
  starting transfers between devices  5.19 us (2%)
    all_gather x1, waiting for transfers between devices, on_device(): portion = lax.all_gather(arrived, 'tp', axis=2, tiled=True)  67 us
    all_to_all x1, blocking collectives, on_device(): lax.all_to_all(padded[owner_of].reshape(expert_count, capacity, moe_rows....  44.2 us
    all_gather x1, waiting for transfers between devices, on_device(): lax.all_gather(hidden, 'tp', axis=2, tiled=True)  27.9 us
    all_gather x1, waiting for transfers between devices, on_device(): lax.all_gather(joined, 'ep', axis=0, tiled=True)  16.9 us
    dot_general x1, matrix products, attend_block(): jnp.einsum('tkgd,skd->kgts', query_rot, keys_part, preferred_element_type...  13.9 us
    unnamed x29, local copies, waits for them, and re-layouts  13.7 us
    reduce_sum x1, other arithmetic, attend_block(): denominator = denominator * factor + jnp.sum(weights, axis=-1)  13.6 us
    dot_general x1, matrix products, attend_block(): jnp.einsum('kgts,skd->kgtd', weights.astype(jnp.bfloat16), values_part, p...  13.6 us
  transfers between devices with their start and end apart: 4, of which 4 were waited for; matrix products, arithmetic and copies ran while one was open for 21% of the time, Pallas kernels for 0%

commit v1 on v0

--- a/solution.py
+++ b/solution.py
@@ -122,7 +122,12 @@
         concat_axis=1,
         tiled=True,
     )
-    portion = lax.all_gather(arrived, "tp", axis=2, tiled=True)
+    ring = [arrived]
+    for hop in range(3):
+        ring.append(lax.ppermute(ring[-1], "tp", [(dev, (dev + 1) % 4) for dev in range(4)]))
+    portion = jnp.roll(
+        jnp.concatenate(ring[::-1], axis=2), (lax.axis_index("tp") + 1) * ring[0].shape[2], axis=2
+    )
     widened = portion.astype(jnp.float32)
     gate_act = jnp.einsum("erd,edf->erf", portion, expert_gate, preferred_element_type=jnp.float32)
     up_act = jnp.einsum("erd,edf->erf", portion, expert_up, preferred_element_type=jnp.float32)

time: 299 us -> 321 us (1.074)
  waiting for transfers between devices: 121 us -> 139 us
  local copies, waits for them, and re-layouts: 29.7 us -> 37.5 us
    ppermute x0 -> x3, waiting for transfers between devices: none -> 103 us  [on_device(): lax.ppermute(ring[-1], 'tp', [(dev, (dev + 1) % 4) for dev in range(4)])]
    all_gather x1 -> x0, waiting for transfers between devices: 67 us -> none  [on_device(): portion = lax.all_gather(arrived, 'tp', axis=2, tiled=True)]
    all_gather x1, waiting for transfers between devices: 16.9 us -> 0.02 us  [on_device(): lax.all_gather(joined, 'ep', axis=0, tiled=True)]
    unnamed x29 -> x34, local copies, waits for them, and re-layouts: 13.7 us -> 20.7 us
  transfers between devices with their start and end apart: 4 -> 6, of which waited for: 4 -> 5; matrix products, arithmetic and copies ran while one was open for 21% -> 20% of each run, Pallas kernels for 0% -> 0%
where the time goes in v1:
time: 321 us; the launch traced here: 317 us
  waiting for transfers between devices  139 us (43%)
  blocking collectives  43.9 us (14%)
  matrix products  41.8 us (13%)
  local copies, waits for them, and re-layouts  37.5 us (12%)
  other arithmetic  33.3 us (10%)
  between operations  14.7 us (5%)
  starting transfers between devices  7.23 us (2%)
    ppermute x3, waiting for transfers between devices, on_device(): lax.ppermute(ring[-1], 'tp', [(dev, (dev + 1) % 4) for dev in range(4)])  103 us
    all_to_all x1, blocking collectives, on_device(): lax.all_to_all(padded[owner_of].reshape(expert_count, capacity, moe_rows....  43.9 us
    all_gather x1, waiting for transfers between devices, on_device(): lax.all_gather(hidden, 'tp', axis=2, tiled=True)  26.1 us
    unnamed x34, local copies, waits for them, and re-layouts  20.7 us
    dot_general x1, matrix products, attend_block(): jnp.einsum('tkgd,skd->kgts', query_rot, keys_part, preferred_element_type...  13.7 us
    reduce_sum x1, other arithmetic, attend_block(): denominator = denominator * factor + jnp.sum(weights, axis=-1)  13.6 us
    dot_general x1, matrix products, attend_block(): jnp.einsum('kgts,skd->kgtd', weights.astype(jnp.bfloat16), values_part, p...  13.6 us
    unnamed x1, other arithmetic  11.2 us
  transfers between devices with their start and end apart: 6, of which 5 were waited for; matrix products, arithmetic and copies ran while one was open for 20% of the time, Pallas kernels for 0%

profile of v1, /device:TPU:0, one launch (start us, length us, event | category | flops | bytes accessed | tf_op | source)
XLA Modules:
  0.0 317.3 jit_solution(8280913886059957763)
XLA Ops:
  9.3 1.1 reduce-window.6
  10.8 2.4 scatter_custom_fusion
  13.3 1.1 concatenate.17
  14.4 2.8 gather_fusion
  17.2 43.9 %all_to_all.21 = bf16[8,96,1024]{2,1,0:T(8,128)(2,1)S(1)} all-to-all(bf16[8,96,1024]{2,1,0:T(8,128)(2,1)S(1)} %bitcast.110), channel_id=1, replica_groups=mesh['ep'=8,'tp'=4] {'ep'}, dimensions={0} | all-to-all | bytes 3145728 | tf_op jit(solution)/shard_map/all_to_all | solution.py:118
  61.2 1.5 collective-permute-start
  62.7 35.2 %collective-permute-done = bf16[1,768,1024]{2,1,0:T(8,128)(2,1)S(1)} collective-permute-done((bf16[1,768,1024]{2,1,0:T(8,128)(2,1)S(1)}, bf16[1,768,1024]{2,1,0:T(8,128)(2,1)S(1)}, u32[]{:S(2)}, u32[]{:S(2)}) %collective-permute-start) | collective-permute-done | bytes 1572896 | tf_op jit(solution)/shard_map/ppermute | solution.py:127
  98.5 35.3 %collective-permute-done.1 = bf16[1,768,1024]{2,1,0:T(8,128)(2,1)} collective-permute-done((bf16[1,768,1024]{2,1,0:T(8,128)(2,1)S(1)}, bf16[1,768,1024]{2,1,0:T(8,128)(2,1)}, u32[]{:S(2)}, u32[]{:S(2)}) %collective-permute-start.1) | collective-permute-done | bytes 1572896 | tf_op jit(solution)/shard_map/ppermute | solution.py:127
  136.4 32.6 %collective-permute-done.2 = bf16[1,768,1024]{2,1,0:T(8,128)(2,1)} collective-permute-done((bf16[1,768,1024]{2,1,0:T(8,128)(2,1)}, bf16[1,768,1024]{2,1,0:T(8,128)(2,1)}, u32[]{:S(2)}, u32[]{:S(2)}) %collective-permute-start.2) | collective-permute-done | bytes 1572896 | tf_op jit(solution)/shard_map/ppermute | solution.py:127
  169.0 1.6 constant_dynamic-update-slice_fusion.7
  170.6 1.6 constant_dynamic-update-slice_fusion.6
  172.5 1.6 constant_dynamic-update-slice_fusion.3
  174.1 1.6 constant_dynamic-update-slice_fusion.2
  176.0 1.3 multiply_reduce_fusion
  178.0 3.4 %fusion.7 = f32[768,512]{1,0:T(8,128)S(1)} fusion(bf16[1,768,8192]{2,1,0:T(8,128)(2,1)S(1)} %constant_dynamic-update-slice_fusion, s32[]{:T(128)S(6)} %select_n.67, bf16[1,4096,512]{2,1,0:T(8,128)(2,1)S(1)} %copy-done.7), kind=kOutput, calls=%fused_computation.12 | convolution fusion | flops 3221225472 | bytes 12058628 | tf_op jit(solution)/shard_map/erd,edf->erf/dot_general | solution.py:132
  181.5 4.5 %multiply_convert_fusion = bf16[768,512]{1,0:T(8,128)(2,1)} fusion(f32[768,512]{1,0:T(8,128)S(1)} %fusion.7, bf16[1,4096,512]{2,1,0:T(8,128)(2,1)S(1)} %copy-done.8, bf16[1,768,8192]{2,1,0:T(8,128)(2,1)S(1)} %constant_dynamic-update-slice_fusion, s32[]{:T(128)S(6)} %select_n.67, f32[768]{0:T(1024)S(1)} %add_rsqrt_fusion.1), kind=kOutput, calls=%fused_computation.23 | convolution fusion | flops 3224371200 | bytes 12849156 | tf_op jit(solution)/shard_map/erd,edf->erf/dot_general | solution.py:133
  187.1 2.7 fusion.48
  189.9 13.7 %bitcast_reduce_fusion = (f32[4,4,256]{2,1,0:T(4,128)S(1)}, f32[4,2048,256,4]{2,1,3,0:T(8,128)}) fusion(bf16[2048,4,64,1]{0,2,3,1:T(8,128)(2,1)S(1)} %bitcast.113, bf16[256,4,4,64]{0,3,2,1:T(8,128)(2,1)S(1)} %bitcast.114), kind=kOutput, calls=%fused_computation.4 | convolution fusion | flops 1090514944 | bytes 35143680 | tf_op jit(solution)/shard_map/tkgd,skd->kgts/dot_general | solution.py:39
  203.6 26.1 %all-gather.6.cloned.1.call-done = bf16[768,2048]{1,0:T(8,128)(2,1)} async-done(((bf16[768,512]{1,0:T(8,128)(2,1)}), bf16[768,2048]{1,0:T(8,128)(2,1)}) %all-gather.6.cloned.1.call-update) | async-done | bytes 3145744 | tf_op jit(solution)/shard_map/all_gather | solution.py:140
  229.7 6.6 %fusion.18 = bf16[1,768,1024]{2,1,0:T(8,128)(2,1)S(1)} fusion(bf16[768,2048]{1,0:T(8,128)(2,1)} %all-gather.6.cloned.1.call-done, bf16[1,2048,1024]{2,1,0:T(8,128)(2,1)} %param.23), kind=kOutput, calls=%fused_computation.24 | convolution fusion | flops 3222011904 | bytes 8912896 | tf_op jit(solution)/shard_map/erf,efd->erd/dot_general | solution.py:138
  236.2 2.4 copy.58
  239.2 11.2 %reduce.3 = bf16[768,1024]{1,0:T(8,128)(2,1)} reduce(bf16[768,1,1024]{2,1,0:T(2,128)(2,1)S(1)} %bitcast.108, bf16[]{:T(256)} %broadcast.330), dimensions={1}, to_apply=%bitcast.101.reduce_sub_computation | reduce | bytes 3145730
  250.4 4.1 %reshape.311 = bf16[8,2,49152]{2,1,0:T(2,128)(2,1)} reshape(bf16[768,1024]{1,0:T(8,128)(2,1)} %reduce.3) | data formatting | bytes 3145728
  254.5 4.6 %all-to-all-start.1 = ((bf16[8,2,49152]{2,1,0:T(2,128)(2,1)}), bf16[8,2,49152]{2,1,0:T(2,128)(2,1)S(1)}, u32[]{:S(2)}, u32[]{:S(2)}) async-start(bf16[8,2,49152]{2,1,0:T(2,128)(2,1)} %reshape.311), calls=%async_computation.1 | async-start | bytes 3145728 | tf_op jit(solution)/shard_map/all_to_all | solution.py:144
  259.1 13.6 %fusion.1 = f32[4,4,256]{2,1,0:T(4,128)S(1)} fusion(f32[4,2048,256,4]{2,1,3,0:T(8,128)} %get-tuple-element.19, f32[4,4,256]{2,1,0:T(4,128)S(1)} %get-tuple-element.18), kind=kLoop, calls=%fused_computation.6 | loop fusion | flops 25161728 | bytes 33587200 | tf_op jit(solution)/shard_map/reduce_sum | solution.py:45
  272.8 13.6 %fusion.34 = bf16[256,4,4,64]{0,3,2,1:T(8,128)(2,1)S(1)} fusion(bf16[2048,4,64,1]{0,2,3,1:T(8,128)(2,1)S(1)} %bitcast.112, f32[4,2048,256,4]{2,1,3,0:T(8,128)} %get-tuple-element.19, f32[4,4,256]{2,1,0:T(4,128)S(1)} %get-tuple-element.18, f32[256,4,4]{0,2,1:T(4,128)S(1)} %bitcast_add_fusion, f32[256,4,4]{0,2,1:T(4,128)S(1)} %multiply_bitcast_fusion), kind=kOutput, calls=%fused_computation.28 | convolution fusion | flops 1099694080 | bytes 35176448 | tf_op jit(solution)/shard_map/kgts,skd->kgtd/dot_general | solution.py:46
  287.4 9.5 %all-to-all-done.1 = bf16[8,2,49152]{2,1,0:T(2,128)(2,1)S(1)} async-done(((bf16[8,2,49152]{2,1,0:T(2,128)(2,1)}), bf16[8,2,49152]{2,1,0:T(2,128)(2,1)S(1)}, u32[]{:S(2)}, u32[]{:S(2)}) %all-to-all-start.1) | async-done | bytes 1572896 | tf_op jit(solution)/shard_map/all_to_all | solution.py:144
  296.9 3.9 %reshape.312 = bf16[768,1,1024]{2,1,0:T(2,128)(2,1)} reshape(bf16[8,2,49152]{2,1,0:T(2,128)(2,1)S(1)} %all-to-all-done.1) | data formatting | bytes 3145728
  300.8 2.5 copy.57
  303.3 2.1 gather_fusion.1
  305.4 1.3 reshape.278
  306.7 3.5 %multiply_reduce_fusion.1 = bf16[256,1024]{1,0:T(8,128)(2,1)} fusion(f32[256,2,1024]{2,1,0:T(2,128)S(1)} %reshape.278, f32[256,2]{1,0:T(8,128)S(1)} %copy.45), kind=kLoop, calls=%fused_computation.20 | loop fusion | flops 786432 | bytes 2623488 | tf_op jit(solution)/shard_map/reduce_sum | solution.py:148
  (72 shorter events, 9.6 us)
Async XLA Ops:
  7.2 180.0 %all-gather.4.cloned.1.call-start = ((), (), s32[]{:S(2)}) async-start(), calls=%async_computation.2 | async-start | bytes 2359296 | tf_op jit(solution)/shard_map/all_gather | solution.py:93
  14.4 119.4 %copy-start.2 = (bf16[256,256]{1,0:T(8,128)(2,1)S(1)}, bf16[256,256]{1,0:T(8,128)(2,1)}, u32[]{:S(2)}) copy-start(bf16[256,256]{1,0:T(8,128)(2,1)} %param.14) | copy-start | bytes 393220
  14.4 120.2 %copy-start.3 = (bf16[256,256]{1,0:T(8,128)(2,1)S(1)}, bf16[256,256]{1,0:T(8,128)(2,1)}, u32[]{:S(2)}) copy-start(bf16[256,256]{1,0:T(8,128)(2,1)} %param.13) | copy-start | bytes 393220
  61.2 36.7 %collective-permute-start = (bf16[1,768,1024]{2,1,0:T(8,128)(2,1)S(1)}, bf16[1,768,1024]{2,1,0:T(8,128)(2,1)S(1)}, u32[]{:S(2)}, u32[]{:S(2)}) collective-permute-start(bf16[1,768,1024]{2,1,0:T(8,128)(2,1)S(1)} %bitcast.105), channel_id=1, source_target_pairs={{0,1},{1,2},{2,3},{3,0},{4,5},{5,6},{6,7},{7,4},{8,9},{9,10},{10,1... | collective-permute-start | bytes 4718600 | tf_op jit(solution)/shard_map/ppermute | solution.py:127
  97.8 35.9 %collective-permute-start.1 = (bf16[1,768,1024]{2,1,0:T(8,128)(2,1)S(1)}, bf16[1,768,1024]{2,1,0:T(8,128)(2,1)}, u32[]{:S(2)}, u32[]{:S(2)}) collective-permute-start(bf16[1,768,1024]{2,1,0:T(8,128)(2,1)S(1)} %collective-permute-done), channel_id=1, source_target_pairs={{0,1},{1,2},{2,3},{3,0},{4,5},{5,6},{6,7},{7,4},{8,9},{9,10},{10,1... | collective-permute-start | bytes 4718600 | tf_op jit(solution)/shard_map/ppermute | solution.py:127
  133.8 35.3 %collective-permute-start.2 = (bf16[1,768,1024]{2,1,0:T(8,128)(2,1)}, bf16[1,768,1024]{2,1,0:T(8,128)(2,1)}, u32[]{:S(2)}, u32[]{:S(2)}) collective-permute-start(bf16[1,768,1024]{2,1,0:T(8,128)(2,1)} %collective-permute-done.1), channel_id=1, source_target_pairs={{0,1},{1,2},{2,3},{3,0},{4,5},{5,6},{6,7},{7,4},{8,9},{9,10},{10,1... | collective-permute-start | bytes 4718600 | tf_op jit(solution)/shard_map/ppermute | solution.py:127
  135.9 93.7 %all-gather.6.cloned.1.call-start = ((), (), s32[]{:S(2)}) async-start(), calls=%async_computation.3 | async-start | bytes 3932160 | tf_op jit(solution)/shard_map/all_gather | solution.py:140
  175.8 2.2 copy-start.7
  178.0 3.4 %copy-start.8 = (bf16[1,4096,512]{2,1,0:T(8,128)(2,1)S(1)}, bf16[1,4096,512]{2,1,0:T(8,128)(2,1)}, u32[]{:S(2)}) copy-start(bf16[1,4096,512]{2,1,0:T(8,128)(2,1)} %param.22) | copy-start | bytes 12582916
  181.4 4.6 %copy-start.6 = (f32[64]{0:T(128)S(1)}, f32[64]{0:T(128)}, u32[]{:S(2)}) copy-start(f32[64]{0:T(128)} %param.15) | copy-start | bytes 772
  181.4 4.7 %copy-start.1 = (bf16[256,1024]{1,0:T(8,128)(2,1)S(1)}, bf16[256,1024]{1,0:T(8,128)(2,1)}, u32[]{:S(2)}) copy-start(bf16[256,1024]{1,0:T(8,128)(2,1)} %param.12) | copy-start | bytes 1572868
  181.4 4.9 %copy-start.4 = (f32[256,2]{0,1:T(2,128)S(1)}, f32[256,2]{0,1:T(2,128)}, u32[]{:S(2)}) copy-start(f32[256,2]{0,1:T(2,128)} %param.20) | copy-start | bytes 6148
  181.5 4.9 %copy-start.5 = (f32[256]{0:T(256)S(1)}, f32[256]{0:T(256)}, u32[]{:S(2)}) copy-start(f32[256]{0:T(256)} %param.19) | copy-start | bytes 3076
  254.5 42.4 %all-to-all-start.1 = ((bf16[8,2,49152]{2,1,0:T(2,128)(2,1)}), bf16[8,2,49152]{2,1,0:T(2,128)(2,1)S(1)}, u32[]{:S(2)}, u32[]{:S(2)}) async-start(bf16[8,2,49152]{2,1,0:T(2,128)(2,1)} %reshape.311), calls=%async_computation.1 | async-start | bytes 3145728 | tf_op jit(solution)/shard_map/all_to_all | solution.py:144
  259.1 13.7 %copy-start = (bf16[2048,256]{0,1:T(8,128)(2,1)S(1)}, bf16[2048,256]{0,1:T(8,128)(2,1)}, u32[]{:S(2)}) copy-start(bf16[2048,256]{0,1:T(8,128)(2,1)} %get-tuple-element.11) | copy-start | bytes 3145732
Sparse Core Ops, SparseCore 0:
  136.0 31.2 all-gather.3
  186.1 43.4 all-gather.5
